TPU v7x, 32 devices: a whole 2x2x4 slice. The times are simulated.
32 devices in a mesh: grp: 2 (over x), ep: 4 (over y, core), tp: 4 (over z).
Axes of the slice: x: 2, y: 2, z: 4, core: 2. Of those that a mesh axis runs over, the one named last changes fastest.
Arguments:
- pool_input: bfloat16 [8192, 1024], P(('grp', 'ep'), 'tp'), parts along dimension 0, may hold values from -6 to 6
- pool_map: bfloat16 [8, 128, 128], replicated, may hold values from -0.5 to 0.5
- pool_scale: float32 [1024], replicated, may hold values from 0.1 to 1.9
- out_weight: bfloat16 [1024, 2048], P(None, 'tp'), may hold values from -0.1875 to 0.1875
- expert_input: bfloat16 [4096, 2048], P(('grp', 'ep', 'tp')), parts along dimension 0, may hold values from -6 to 6
- norm_gain: float32 [2048], replicated, may hold values from 0.1 to 1.9
- routes: int32 [4096, 2], P(('grp', 'ep', 'tp')), parts along dimension 0, may hold values from 0 to 15, all different within a row; in each aligned block of 128 rows (0 to 127, 128 to 255, ...) at most 32 rows name the same one
- route_weight: float32 [4096, 2], P(('grp', 'ep', 'tp')), parts along dimension 0, may hold values from 0.2 to 1.5
- gate_weight: bfloat16 [16, 2048, 512], P(('ep', 'tp')), may hold values from -0.125 to 0.125
- up_weight: bfloat16 [16, 2048, 512], P(('ep', 'tp')), may hold values from -0.125 to 0.125
- down_weight: bfloat16 [16, 512, 2048], P(('ep', 'tp')), may hold values from -0.25 to 0.25
Outputs:
- pool_output: bfloat16 [8192, 2048], P(('grp', 'ep'), 'tp'), parts along dimension 0
- expert_output: bfloat16 [4096, 2048], P(('grp', 'ep', 'tp')), parts along dimension 0
There are 2 independent parts, one for each index of `grp`. A program takes and returns all parts, laid end to end along the dimension named above; an argument that names none is the same for every part. Nothing has to cross between parts.
Inputs may be any that keep to these rules, and one draw needn't show every extreme that they name: `routes`: each row names 2 different experts. In the rows of one device no expert is named more than 32 times, and in every draw some device names some expert exactly 32 times.
All inputs are finite; a program needn't handle non-finite values.
Results may differ from a plain program's by a relative error of at most 0.007.
Values may be sent and summed in bfloat16 or wider, within the bound.
No kernel may reach another device: no remote copies, remote signals or barrier semaphores. Data moves between devices by JAX's collectives and lax.ppermute only.
A program may use at most 64 MiB of HBM per device.

v0:
```python
import jax
import jax.numpy as jnp
from jax import lax
from jax.sharding import PartitionSpec as P

epsilon = 1e-06
halo_depth = 16


def shifted_2(shard, axis, by):
    size = lax.axis_size(axis)
    pairs = [(i, i + by) for i in range(size) if 0 <= i + by < size]
    return lax.ppermute(shard, axis, pairs)


def expert_rows(received, gate_weight, up_weight, down_weight):
    shape_in = received.shape
    flat_rows = received.reshape(-1, shape_in[-1])
    gate_part = jnp.dot(flat_rows, gate_weight[0], preferred_element_type=jnp.float32)
    up_part = jnp.dot(flat_rows, up_weight[0], preferred_element_type=jnp.float32)
    hidden = (jax.nn.silu(gate_part) * up_part).astype(jnp.bfloat16)
    result = jnp.dot(hidden, down_weight[0], preferred_element_type=jnp.float32).astype(
        jnp.bfloat16
    )
    return result.reshape(shape_in)


def pool_half(pool_input, pool_map, pool_scale, out_weight):
    row_count, width_local = pool_input.shape
    group_dim = pool_map.shape[1]
    groups_local = width_local // group_dim
    last_rows = pool_input[row_count - halo_depth :]
    earlier_rows = shifted_2(last_rows, "ep", 1)
    extended = jnp.concatenate([earlier_rows, pool_input], axis=0).astype(jnp.float32)
    first_group = lax.axis_index("tp") * groups_local
    group_ids = first_group + jnp.arange(width_local, dtype=jnp.int32) // group_dim
    window = jnp.left_shift(jnp.int32(2), group_ids % 4)
    summed = jnp.zeros((row_count, width_local), jnp.float32)
    for offset in range(halo_depth):
        shifted = extended[halo_depth - offset : halo_depth - offset + row_count]
        summed = summed + jnp.where(offset < window, shifted, 0.0)
    positions = lax.axis_index("ep") * row_count + jnp.arange(row_count, dtype=jnp.int32)
    counted = jnp.minimum(positions[:, None] + 1, window[None, :]).astype(jnp.float32)
    pooled = (summed / counted - extended[halo_depth:]).astype(jnp.bfloat16)
    maps_local = lax.dynamic_slice_in_dim(pool_map, first_group, groups_local, 0)
    scales_local = lax.dynamic_slice_in_dim(pool_scale, first_group * group_dim, width_local, 0)
    mapped = jnp.einsum(
        "rgc,gcd->rgd",
        pooled.reshape(row_count, groups_local, group_dim),
        maps_local,
        preferred_element_type=jnp.float32,
    )
    mapped = (mapped.reshape(row_count, width_local) * scales_local).astype(jnp.bfloat16)
    projected = jnp.dot(
        lax.all_gather(mapped, "tp", axis=1, tiled=True),
        out_weight,
        preferred_element_type=jnp.float32,
    )
    return projected.astype(jnp.bfloat16)


def expert_half(expert_input, norm_gain, routes, route_weight, gate_weight, up_weight, down_weight):
    row_count, model_width = expert_input.shape
    top_count = routes.shape[1]
    widened = expert_input.astype(jnp.float32)
    normed = (
        widened
        * lax.rsqrt(jnp.mean(widened * widened, axis=1, keepdims=True) + epsilon)
        * norm_gain
    )
    normed = normed.astype(jnp.bfloat16)
    ep_count = lax.axis_size("ep")
    tp_count = lax.axis_size("tp")
    experts = ep_count * tp_count
    capacity = 2 * row_count * top_count // experts
    copies = row_count * top_count
    flat_routes = routes.reshape(copies)
    onehot = (flat_routes[:, None] == jnp.arange(experts, dtype=jnp.int32)[None, :]).astype(
        jnp.int32
    )
    slot_index = jnp.sum((jnp.cumsum(onehot, axis=0) - onehot) * onehot, axis=1)
    target = flat_routes * capacity + slot_index
    source_row = jnp.arange(copies, dtype=jnp.int32) // top_count
    slot_table = jnp.full((experts * capacity,), row_count, jnp.int32).at[target].set(source_row)
    padded = jnp.concatenate([normed, jnp.zeros((1, model_width), jnp.bfloat16)], axis=0)
    outgoing = padded[slot_table].reshape(experts, capacity, model_width)
    results = expert_rows(
        lax.all_to_all(outgoing, ("ep", "tp"), split_axis=0, concat_axis=0, tiled=True),
        gate_weight,
        up_weight,
        down_weight,
    )
    returned = lax.all_to_all(results, ("ep", "tp"), split_axis=0, concat_axis=0, tiled=True)
    returned = returned.reshape(experts * capacity, model_width)
    picked = returned[target].astype(jnp.float32) * route_weight.reshape(copies)[:, None]
    return picked.reshape(row_count, top_count, model_width).sum(axis=1).astype(jnp.bfloat16)


def on_device(
    pool_input,
    pool_map,
    pool_scale,
    out_weight,
    expert_input,
    norm_gain,
    routes,
    route_weight,
    gate_weight,
    up_weight,
    down_weight,
):
    pool_output = pool_half(pool_input, pool_map, pool_scale, out_weight)
    expert_output = expert_half(
        expert_input, norm_gain, routes, route_weight, gate_weight, up_weight, down_weight
    )
    return (pool_output, expert_output)


def solution(mesh):
    return jax.shard_map(
        on_device,
        mesh=mesh,
        in_specs=(
            P(("grp", "ep"), "tp"),
            P(),
            P(),
            P(None, "tp"),
            P(("grp", "ep", "tp"), None),
            P(),
            P(("grp", "ep", "tp"), None),
            P(("grp", "ep", "tp"), None),
            P(("ep", "tp"), None, None),
            P(("ep", "tp"), None, None),
            P(("ep", "tp"), None, None),
        ),
        out_specs=(P(("grp", "ep"), "tp"), P(("grp", "ep", "tp"), None)),
        check_vma=False,
    )
```

profile of v0, /device:TPU:0, one launch (start us, length us, event | category | flops | bytes accessed | tf_op | source)
XLA Modules:
  0.0 192.7 jit_solution(14643236694304669269)
XLA Ops:
  7.2 0.9 copy.19
  8.1 0.1 eq.31
  8.3 0.1 eq.27
  8.4 0.7 broadcast_multiply_fusion
  9.1 0.6 reduce-window.6
  9.7 0.2 slice_reduce_fusion
  9.9 0.1 copy.18
  10.0 0.1 mul.83
  10.2 0.1 fusion.43
  10.3 1.4 scatter_custom_fusion
  11.7 1.2 fusion.11
  12.9 1.2 fusion.13
  14.2 3.3 %gather_fusion = bf16[512,2048]{1,0:T(8,128)(2,1)} fusion(bf16[129,2048]{1,0:T(8,128)(2,1)S(1)} %concatenate.7, s32[1024]{0:T(1024)S(1)} %pad_clamp_fusion.1), kind=kCustom, calls=%fused_computation | custom fusion | bytes 4196352 | tf_op jit(solution)/shard_map/gather | solution.py:86
  17.6 7.5 %all-to-all-start = ((bf16[16,32,2048]{2,1,0:T(8,128)(2,1)}), bf16[16,32,2048]{2,1,0:T(8,128)(2,1)}, u32[]{:S(2)}, u32[]{:S(2)}) async-start(bf16[16,32,2048]{2,1,0:T(8,128)(2,1)} %bitcast.57), calls=%async_computation | async-start | bytes 4194304 | tf_op jit(solution)/shard_map/all_to_all | solution.py:88
  25.0 0.7 slice.58
  25.8 2.2 %collective-permute-start = (bf16[16,256]{1,0:T(8,128)(2,1)S(1)}, bf16[16,256]{1,0:T(8,128)(2,1)S(1)}, u32[]{:S(2)}, u32[]{:S(2)}) collective-permute-start(bf16[16,256]{1,0:T(8,128)(2,1)S(1)} %slice.58), channel_id=1, source_target_pairs={{0,4},{4,8},{8,12},{1,5},{5,9},{9,13},{2,6},{6,10},{10,14},{3,7},{... | collective-permute-start | bytes 24584 | tf_op jit(solution)/shard_map/ppermute | solution.py:13
  28.2 0.8 dynamic_slice.7
  29.0 1.1 maximum_convert_fusion
  30.1 44.3 %all-to-all-done = bf16[16,32,2048]{2,1,0:T(8,128)(2,1)} async-done(((bf16[16,32,2048]{2,1,0:T(8,128)(2,1)}), bf16[16,32,2048]{2,1,0:T(8,128)(2,1)}, u32[]{:S(2)}, u32[]{:S(2)}) %all-to-all-start) | async-done | bytes 2097184 | tf_op jit(solution)/shard_map/all_to_all | solution.py:88
  74.4 4.4 %fusion.3 = f32[512,512]{1,0:T(8,128)} fusion(bf16[512,2048]{1,0:T(8,128)(2,1)} %bitcast.6, bf16[1,2048,512]{2,1,0:T(8,128)(2,1)} %param.19), kind=kOutput, calls=%fused_computation.7 | convolution fusion | flops 1073741824 | bytes 5242880 | tf_op jit(solution)/shard_map/dot_general | solution.py:19
  78.9 6.3 %convolution_convert_fusion = bf16[512,2048]{1,0:T(8,128)(2,1)} fusion(bf16[1,512,2048]{2,1,0:T(8,128)(2,1)S(1)} %copy-done, bf16[512,2048]{1,0:T(8,128)(2,1)} %bitcast.6, bf16[1,2048,512]{2,1,0:T(8,128)(2,1)} %param.20, f32[512,512]{1,0:T(8,128)} %fusion.3), kind=kOutput, calls=%fused_computation.3 | convolution fusion | flops 2150105088 | bytes 9437184 | tf_op jit(solution)/shard_map/dot_general | solution.py:22
  85.1 4.4 %all-to-all-start.1 = ((bf16[16,32,2048]{2,1,0:T(8,128)(2,1)}), bf16[16,32,2048]{2,1,0:T(8,128)(2,1)}, u32[]{:S(2)}, u32[]{:S(2)}) async-start(bf16[16,32,2048]{2,1,0:T(8,128)(2,1)} %bitcast.58), calls=%async_computation.1 | async-start | bytes 4194304 | tf_op jit(solution)/shard_map/all_to_all | solution.py:93
  89.6 0.2 all-gather.2.cloned.1.call-start
  89.8 3.8 %fusion.35 = f32[2,128,1024]{2,1,0:T(8,128)S(1)} fusion(bf16[8,128,128]{2,1,0:T(8,128)(2,1)} %param.12, s32[]{:T(128)S(6)} %select_n.92, s32[256]{0:T(256)S(1)} %fusion.46, s32[1024]{0:T(1024)S(1)} %add_add_fusion, f32[1040,256]{1,0:T(8,128)S(1)} %maximum_convert_fusion, pred[256]{0:T(512)(128)(4,1)S(1)} %get-tuple-element.2, ...), kind=kOutput, calls=%fused_computation.54 | convolution fusion | flops 76546048 | bytes 17904644 | tf_op jit(solution)/shard_map/rgc,gcd->rgd/dot_general | solution.py:47
  93.7 0.9 fusion.31
  94.6 0.0 all-gather.2.cloned.1.call-update
  94.6 0.1 copy.22
  94.8 75.0 %all-gather.2.cloned.1.call-done = bf16[1024,1024]{0,1:T(8,128)(2,1)} async-done(((bf16[1024,256]{0,1:T(8,128)(2,1)}), bf16[1024,1024]{0,1:T(8,128)(2,1)}) %all-gather.2.cloned.1.call-update) | async-done | bytes 2097168 | tf_op jit(solution)/shard_map/all_gather | solution.py:55
  169.8 3.9 %convolution_convert_fusion.1 = bf16[1024,512]{1,0:T(8,128)(2,1)} fusion(bf16[1024,1024]{0,1:T(8,128)(2,1)} %all-gather.2.cloned.1.call-done, bf16[1024,512]{1,0:T(8,128)(2,1)S(1)} %copy-done.2), kind=kOutput, calls=%fused_computation.10 | convolution fusion | flops 1074266112 | bytes 4194304 | tf_op jit(solution)/shard_map/dot_general | solution.py:54
  173.6 4.2 %gather_fusion.1 = bf16[256,2048]{1,0:T(8,128)(2,1)S(1)} fusion(bf16[512,2048]{1,0:T(8,128)(2,1)} %bitcast.11, s32[1024]{0:T(1024)S(1)} %pad_clamp_fusion), kind=kCustom, calls=%fused_computation.1 | custom fusion | bytes 2098176 | tf_op jit(solution)/shard_map/gather | solution.py:95
  177.9 2.4 %reshape.127 = f32[128,2,2048]{2,1,0:T(2,128)} reshape(bf16[256,2048]{1,0:T(8,128)(2,1)S(1)} %gather_fusion.1) | data formatting | bytes 3145728 | tf_op jit(solution)/shard_map/convert_element_type | solution.py:95
  180.2 5.6 %multiply_reduce_fusion = bf16[128,2048]{1,0:T(8,128)(2,1)} fusion(f32[128,2,2048]{2,1,0:T(2,128)} %reshape.127, f32[128,2]{1,0:T(8,128)S(1)} %copy.22), kind=kLoop, calls=%fused_computation.9 | loop fusion | flops 786432 | bytes 2622464 | tf_op jit(solution)/shard_map/reduce_sum | solution.py:96
  (28 shorter events, 0.3 us)
Async XLA Ops:
  7.2 71.7 %copy-start = (bf16[1,512,2048]{2,1,0:T(8,128)(2,1)S(1)}, bf16[1,512,2048]{2,1,0:T(8,128)(2,1)}, u32[]{:S(2)}) copy-start(bf16[1,512,2048]{2,1,0:T(8,128)(2,1)} %param.21) | copy-start | bytes 6291460
  17.6 56.8 %all-to-all-start = ((bf16[16,32,2048]{2,1,0:T(8,128)(2,1)}), bf16[16,32,2048]{2,1,0:T(8,128)(2,1)}, u32[]{:S(2)}, u32[]{:S(2)}) async-start(bf16[16,32,2048]{2,1,0:T(8,128)(2,1)} %bitcast.57), calls=%async_computation | async-start | bytes 4194304 | tf_op jit(solution)/shard_map/all_to_all | solution.py:88
  25.8 3.2 %collective-permute-start = (bf16[16,256]{1,0:T(8,128)(2,1)S(1)}, bf16[16,256]{1,0:T(8,128)(2,1)S(1)}, u32[]{:S(2)}, u32[]{:S(2)}) collective-permute-start(bf16[16,256]{1,0:T(8,128)(2,1)S(1)} %slice.58), channel_id=1, source_target_pairs={{0,4},{4,8},{8,12},{1,5},{5,9},{9,13},{2,6},{6,10},{10,14},{3,7},{... | collective-permute-start | bytes 24584 | tf_op jit(solution)/shard_map/ppermute | solution.py:13
  85.1 88.5 %all-to-all-start.1 = ((bf16[16,32,2048]{2,1,0:T(8,128)(2,1)}), bf16[16,32,2048]{2,1,0:T(8,128)(2,1)}, u32[]{:S(2)}, u32[]{:S(2)}) async-start(bf16[16,32,2048]{2,1,0:T(8,128)(2,1)} %bitcast.58), calls=%async_computation.1 | async-start | bytes 4194304 | tf_op jit(solution)/shard_map/all_to_all | solution.py:93
  89.6 80.2 %all-gather.2.cloned.1.call-start = ((), (), s32[]{:S(2)}) async-start(), calls=%async_computation.2 | async-start | bytes 2621440 | tf_op jit(solution)/shard_map/all_gather | solution.py:55
  93.7 1.0 copy-start.1
  93.7 76.1 %copy-start.2 = (bf16[1024,512]{1,0:T(8,128)(2,1)S(1)}, bf16[1024,512]{1,0:T(8,128)(2,1)}, u32[]{:S(2)}) copy-start(bf16[1024,512]{1,0:T(8,128)(2,1)} %param.14) | copy-start | bytes 3145732
Sparse Core Ops, SparseCore 0:
  94.7 74.9 all-gather.1
where the time goes:
time: 193 us
  waiting for transfers between devices  119 us (62%)
  matrix products  18.4 us (10%)
  local copies, waits for them, and re-layouts  14.6 us (8%)
  starting transfers between devices  14.4 us (7%)
  between operations  14.2 us (7%)
  other arithmetic  11.7 us (6%)
    all_gather x1, waiting for transfers between devices, pool_half(): lax.all_gather(mapped, 'tp', axis=1, tiled=True)  75 us
    all_to_all x1, waiting for transfers between devices, expert_half(): lax.all_to_all(outgoing, ('ep', 'tp'), split_axis=0, concat_axis=0, tiled...  44.3 us
    all_to_all x1, starting transfers between devices, expert_half(): lax.all_to_all(outgoing, ('ep', 'tp'), split_axis=0, concat_axis=0, tiled...  7.46 us
    dot_general x1, matrix products, expert_rows(): jnp.dot(hidden, down_weight[0], preferred_element_type=jnp.float32)  6.28 us
    reduce_sum x1, other arithmetic, expert_half(): picked.reshape(row_count, top_count, model_width).sum(axis=1)  5.59 us
    dot_general x1, matrix products, expert_rows(): jnp.dot(flat_rows, gate_weight[0], preferred_element_type=jnp.float32)  4.44 us
    all_to_all x1, starting transfers between devices, expert_half(): lax.all_to_all(results, ('ep', 'tp'), split_axis=0, concat_axis=0, tiled=...  4.44 us
    gather x1, local copies, waits for them, and re-layouts, expert_half(): returned[target].astype(jnp.float32) * route_weight.reshape(copies)[:, None]  4.22 us
  transfers between devices with their start and end apart: 4, of which 2 were waited for; matrix products, arithmetic and copies ran while one was open for 6% of the time, Pallas kernels for 0%

commit v1 on v0

--- a/solution.py
+++ b/solution.py
@@ -51,11 +51,8 @@
         preferred_element_type=jnp.float32,
     )
     mapped = (mapped.reshape(row_count, width_local) * scales_local).astype(jnp.bfloat16)
-    projected = jnp.dot(
-        lax.all_gather(mapped, "tp", axis=1, tiled=True),
-        out_weight,
-        preferred_element_type=jnp.float32,
-    )
+    check_stages_all = lambda work_x: jnp.concatenate(jax.lax.all_gather(work_x, axis_name="tp"), 1)
+    projected = jnp.dot(check_stages_all(mapped), out_weight, preferred_element_type=jnp.float32)
     return projected.astype(jnp.bfloat16)
 
 

time: 193 us -> 198 us (1.026)
  local copies, waits for them, and re-layouts: 14.6 us -> 20.2 us
  waiting for transfers between devices: 119 us -> 117 us
    all_gather x0 -> x1, local copies, waits for them, and re-layouts: none -> 3.98 us  [pool_half(): jax.lax.all_gather(work_x, axis_name='tp')]
    all_gather x1, waiting for transfers between devices: 75 us -> 73 us  [pool_half(): jax.lax.all_gather(work_x, axis_name='tp')]
  transfers between devices with their start and end apart: 4 -> 4, of which waited for: 2 -> 2; matrix products, arithmetic and copies ran while one was open for 6% -> 9% of each run, Pallas kernels for 0% -> 0%
where the time goes in v1:
time: 198 us
  waiting for transfers between devices  117 us (59%)
  local copies, waits for them, and re-layouts  20.2 us (10%)
  matrix products  19.8 us (10%)
  starting transfers between devices  14.4 us (7%)
  between operations  14.2 us (7%)
  other arithmetic  11.6 us (6%)
    all_gather x1, waiting for transfers between devices, pool_half(): jax.lax.all_gather(work_x, axis_name='tp')  73 us
    all_to_all x1, waiting for transfers between devices, expert_half(): lax.all_to_all(outgoing, ('ep', 'tp'), split_axis=0, concat_axis=0, tiled...  44.3 us
    all_to_all x1, starting transfers between devices, expert_half(): lax.all_to_all(outgoing, ('ep', 'tp'), split_axis=0, concat_axis=0, tiled...  7.46 us
    dot_general x1, matrix products, expert_rows(): jnp.dot(hidden, down_weight[0], preferred_element_type=jnp.float32)  6.28 us
    reduce_sum x1, other arithmetic, expert_half(): picked.reshape(row_count, top_count, model_width).sum(axis=1)  5.59 us
    dot_general x1, matrix products, pool_half(): jnp.einsum('rgc,gcd->rgd', pooled.reshape(row_count, groups_local, group_...  5.25 us
    dot_general x1, matrix products, expert_rows(): jnp.dot(flat_rows, gate_weight[0], preferred_element_type=jnp.float32)  4.44 us
    all_to_all x1, starting transfers between devices, expert_half(): lax.all_to_all(results, ('ep', 'tp'), split_axis=0, concat_axis=0, tiled=...  4.44 us
  transfers between devices with their start and end apart: 4, of which 2 were waited for; matrix products, arithmetic and copies ran while one was open for 9% of the time, Pallas kernels for 0%

profile of v1, /device:TPU:0, one launch (start us, length us, event | category | flops | bytes accessed | tf_op | source)
XLA Modules:
  0.0 197.5 jit_solution(8453248180965165333)
XLA Ops:
  7.2 0.9 copy.36
  8.1 0.1 eq.31
  8.3 0.1 eq.27
  8.4 0.7 broadcast_multiply_fusion
  9.1 0.6 reduce-window.6
  9.7 0.2 slice_reduce_fusion
  9.9 0.1 copy.35
  10.0 0.1 mul.90
  10.3 1.4 scatter_custom_fusion
  11.7 1.2 fusion.11
  12.9 1.2 fusion.13
  14.2 3.3 %gather_fusion = bf16[512,2048]{1,0:T(8,128)(2,1)} fusion(bf16[129,2048]{1,0:T(8,128)(2,1)S(1)} %concatenate.7, s32[1024]{0:T(1024)S(1)} %pad_clamp_fusion.1), kind=kCustom, calls=%fused_computation | custom fusion | bytes 4196352 | tf_op jit(solution)/shard_map/gather | solution.py:83
  17.6 7.5 %all-to-all-start = ((bf16[16,32,2048]{2,1,0:T(8,128)(2,1)}), bf16[16,32,2048]{2,1,0:T(8,128)(2,1)}, u32[]{:S(2)}, u32[]{:S(2)}) async-start(bf16[16,32,2048]{2,1,0:T(8,128)(2,1)} %bitcast.57), calls=%async_computation | async-start | bytes 4194304 | tf_op jit(solution)/shard_map/all_to_all | solution.py:85
  25.0 0.7 slice.58
  25.8 2.2 %collective-permute-start = (bf16[16,256]{1,0:T(8,128)(2,1)S(1)}, bf16[16,256]{1,0:T(8,128)(2,1)S(1)}, u32[]{:S(2)}, u32[]{:S(2)}) collective-permute-start(bf16[16,256]{1,0:T(8,128)(2,1)S(1)} %slice.58), channel_id=1, source_target_pairs={{0,4},{4,8},{8,12},{1,5},{5,9},{9,13},{2,6},{6,10},{10,14},{3,7},{... | collective-permute-start | bytes 24584 | tf_op jit(solution)/shard_map/ppermute | solution.py:13
  28.2 0.8 dynamic_slice.7
  29.0 1.1 maximum_convert_fusion
  30.1 44.3 %all-to-all-done = bf16[16,32,2048]{2,1,0:T(8,128)(2,1)} async-done(((bf16[16,32,2048]{2,1,0:T(8,128)(2,1)}), bf16[16,32,2048]{2,1,0:T(8,128)(2,1)}, u32[]{:S(2)}, u32[]{:S(2)}) %all-to-all-start) | async-done | bytes 2097184 | tf_op jit(solution)/shard_map/all_to_all | solution.py:85
  74.4 4.4 %fusion.3 = f32[512,512]{1,0:T(8,128)} fusion(bf16[512,2048]{1,0:T(8,128)(2,1)} %bitcast.8, bf16[1,2048,512]{2,1,0:T(8,128)(2,1)} %param.19), kind=kOutput, calls=%fused_computation.7 | convolution fusion | flops 1073741824 | bytes 5242880 | tf_op jit(solution)/shard_map/dot_general | solution.py:19
  78.9 6.3 %convolution_convert_fusion = bf16[512,2048]{1,0:T(8,128)(2,1)} fusion(bf16[1,512,2048]{2,1,0:T(8,128)(2,1)S(1)} %copy-done, bf16[512,2048]{1,0:T(8,128)(2,1)} %bitcast.8, bf16[1,2048,512]{2,1,0:T(8,128)(2,1)} %param.20, f32[512,512]{1,0:T(8,128)} %fusion.3), kind=kOutput, calls=%fused_computation.3 | convolution fusion | flops 2150105088 | bytes 9437184 | tf_op jit(solution)/shard_map/dot_general | solution.py:22
  85.1 4.4 %all-to-all-start.1 = ((bf16[16,32,2048]{2,1,0:T(8,128)(2,1)}), bf16[16,32,2048]{2,1,0:T(8,128)(2,1)}, u32[]{:S(2)}, u32[]{:S(2)}) async-start(bf16[16,32,2048]{2,1,0:T(8,128)(2,1)} %bitcast.58), calls=%async_computation.1 | async-start | bytes 4194304 | tf_op jit(solution)/shard_map/all_to_all | solution.py:90
  89.6 0.2 all-gather.2.cloned.1.call-start
  89.8 5.3 %fusion.34 = f32[2,128,1024]{2,1,0:T(8,128)} fusion(bf16[8,128,128]{2,1,0:T(8,128)(2,1)} %param.12, s32[]{:T(128)S(6)} %select_n.92, s32[256]{0:T(256)S(1)} %fusion.45, s32[1024]{0:T(1024)S(1)} %add_add_fusion, f32[1040,256]{1,0:T(8,128)S(1)} %maximum_convert_fusion, pred[256]{0:T(512)(128)(4,1)S(1)} %get-tuple-element.2, ...), kind=kOutput, calls=%fused_computation.53 | convolution fusion | flops 76546048 | bytes 17904644 | tf_op jit(solution)/shard_map/rgc,gcd->rgd/dot_general | solution.py:47
  95.1 1.6 copy.33
  96.6 0.9 multiply_convert_fusion
  97.5 0.1 copy.39
  97.7 73.0 %all-gather.2.cloned.1.call-done = bf16[4,1024,256]{2,1,0:T(8,128)(2,1)} async-done(((bf16[1,1024,256]{2,1,0:T(8,128)(2,1)}), bf16[4,1024,256]{2,1,0:T(8,128)(2,1)}) %all-gather.2.cloned.1.call-update) | async-done | bytes 2097168 | tf_op jit(solution)/shard_map/all_gather | solution.py:54
  170.7 4.0 %copy.34 = bf16[4,1024,256]{1,2,0:T(8,128)(2,1)} copy(bf16[4,1024,256]{2,1,0:T(8,128)(2,1)} %all-gather.2.cloned.1.call-done) | data formatting | bytes 4194304 | tf_op jit(solution)/shard_map/all_gather | solution.py:54
  174.6 3.9 %convolution_convert_fusion.1 = bf16[1024,512]{1,0:T(8,128)(2,1)} fusion(bf16[1024,1024]{0,1:T(8,128)(2,1)} %bitcast.59, bf16[1024,512]{1,0:T(8,128)(2,1)S(1)} %copy-done.2), kind=kOutput, calls=%fused_computation.10 | convolution fusion | flops 1074266112 | bytes 4194304 | tf_op jit(solution)/shard_map/dot_general | solution.py:55
  178.5 4.2 %gather_fusion.1 = bf16[256,2048]{1,0:T(8,128)(2,1)S(1)} fusion(bf16[512,2048]{1,0:T(8,128)(2,1)} %bitcast.13, s32[1024]{0:T(1024)S(1)} %pad_clamp_fusion), kind=kCustom, calls=%fused_computation.1 | custom fusion | bytes 2098176 | tf_op jit(solution)/shard_map/gather | solution.py:92
  182.7 2.4 %reshape.169 = f32[128,2,2048]{2,1,0:T(2,128)} reshape(bf16[256,2048]{1,0:T(8,128)(2,1)S(1)} %gather_fusion.1) | data formatting | bytes 3145728 | tf_op jit(solution)/shard_map/convert_element_type | solution.py:92
  185.1 5.6 %multiply_reduce_fusion = bf16[128,2048]{1,0:T(8,128)(2,1)} fusion(f32[128,2,2048]{2,1,0:T(2,128)} %reshape.169, f32[128,2]{1,0:T(8,128)S(1)} %copy.39), kind=kLoop, calls=%fused_computation.9 | loop fusion | flops 786432 | bytes 2622464 | tf_op jit(solution)/shard_map/reduce_sum | solution.py:93
  (30 shorter events, 0.4 us)
Async XLA Ops:
  7.2 71.7 %copy-start = (bf16[1,512,2048]{2,1,0:T(8,128)(2,1)S(1)}, bf16[1,512,2048]{2,1,0:T(8,128)(2,1)}, u32[]{:S(2)}) copy-start(bf16[1,512,2048]{2,1,0:T(8,128)(2,1)} %param.21) | copy-start | bytes 6291460
  17.6 56.8 %all-to-all-start = ((bf16[16,32,2048]{2,1,0:T(8,128)(2,1)}), bf16[16,32,2048]{2,1,0:T(8,128)(2,1)}, u32[]{:S(2)}, u32[]{:S(2)}) async-start(bf16[16,32,2048]{2,1,0:T(8,128)(2,1)} %bitcast.57), calls=%async_computation | async-start | bytes 4194304 | tf_op jit(solution)/shard_map/all_to_all | solution.py:85
  25.8 3.2 %collective-permute-start = (bf16[16,256]{1,0:T(8,128)(2,1)S(1)}, bf16[16,256]{1,0:T(8,128)(2,1)S(1)}, u32[]{:S(2)}, u32[]{:S(2)}) collective-permute-start(bf16[16,256]{1,0:T(8,128)(2,1)S(1)} %slice.58), channel_id=1, source_target_pairs={{0,4},{4,8},{8,12},{1,5},{5,9},{9,13},{2,6},{6,10},{10,14},{3,7},{... | collective-permute-start | bytes 24584 | tf_op jit(solution)/shard_map/ppermute | solution.py:13
  85.1 93.4 %all-to-all-start.1 = ((bf16[16,32,2048]{2,1,0:T(8,128)(2,1)}), bf16[16,32,2048]{2,1,0:T(8,128)(2,1)}, u32[]{:S(2)}, u32[]{:S(2)}) async-start(bf16[16,32,2048]{2,1,0:T(8,128)(2,1)} %bitcast.58), calls=%async_computation.1 | async-start | bytes 4194304 | tf_op jit(solution)/shard_map/all_to_all | solution.py:90
  89.6 81.1 %all-gather.2.cloned.1.call-start = ((), (), s32[]{:S(2)}) async-start(), calls=%async_computation.2 | async-start | bytes 2621440 | tf_op jit(solution)/shard_map/all_gather | solution.py:54
  95.1 2.5 %copy-start.1 = (f32[128,2]{0,1:T(2,128)S(1)}, f32[128,2]{0,1:T(2,128)}, u32[]{:S(2)}) copy-start(f32[128,2]{0,1:T(2,128)} %param.18) | copy-start | bytes 3076
  97.7 77.0 %copy-start.2 = (bf16[1024,512]{1,0:T(8,128)(2,1)S(1)}, bf16[1024,512]{1,0:T(8,128)(2,1)}, u32[]{:S(2)}) copy-start(bf16[1024,512]{1,0:T(8,128)(2,1)} %param.14) | copy-start | bytes 3145732
Sparse Core Ops, SparseCore 0:
  97.7 72.9 all-gather.1
